TPU v7x, 512 devices: a whole 4x4x16 slice. The times are simulated.
512 devices in a mesh: kv: 64 (over z, y), tp: 8 (over x, core).
Axes of the slice: x: 4, y: 4, z: 16, core: 2. Of those that a mesh axis runs over, the one named last changes fastest.
Arguments:
- tokens: bfloat16 [256, 4096], P(None, 'kv')
- lengths: int32 [64], replicated, may hold values from 1 to 4, 112 in all
- memory: float32 [64, 16, 128, 128], P('kv', 'tp'), may hold values from -0.6 to 0.6
- norm_gain: float32 [4096], P('kv'), may hold values from 0.1 to 1.9
- w_query: bfloat16 [4096, 2048], P('kv', 'tp'), may hold values from -0.09375 to 0.09375
- w_key: bfloat16 [4096, 2048], P('kv', 'tp'), may hold values from -0.09375 to 0.09375
- w_value: bfloat16 [4096, 2048], P('kv', 'tp'), may hold values from -0.09375 to 0.09375
- w_outgate: bfloat16 [4096, 2048], P('kv', 'tp'), may hold values from -0.09375 to 0.09375
- w_alpha: bfloat16 [4096, 16], P('kv'), may hold values from -0.09375 to 0.09375
- w_beta: bfloat16 [4096, 16], P('kv'), may hold values from -0.09375 to 0.09375
- decay_log: float32 [16], P('tp'), may hold values from -4 to 0.5
- decay_bias: float32 [16], P('tp'), may hold values from -1 to 1
- head_gain: float32 [128], replicated, may hold values from 0.1 to 1.9
- w_output: bfloat16 [2048, 4096], P('tp', 'kv'), may hold values from -0.125 to 0.125
- mlp_gain: float32 [4096], P('kv'), may hold values from 0.1 to 1.9
- w_gate: bfloat16 [4096, 11264], P('kv', 'tp'), may hold values from -0.09375 to 0.09375
- w_up: bfloat16 [4096, 11264], P('kv', 'tp'), may hold values from -0.09375 to 0.09375
- w_down: bfloat16 [11264, 4096], P('tp', 'kv'), may hold values from -0.0546875 to 0.0546875
Outputs:
- layer_out: bfloat16 [256, 4096], P(None, 'kv')
- new_memory: float32 [64, 16, 128, 128], P('kv', 'tp')
Inputs may be any that keep to these rules, and one draw needn't show every extreme that they name: How many of a sequence's 4 slots hold live tokens; the live ones come first; the lengths add up to seven quarters of 64, rounded down.
All inputs are finite; a program needn't handle non-finite values.
Results may differ from a plain program's by a relative error of at most 0.012.
Values may be sent and summed in bfloat16 or wider, within the bound.
A program may use at most 64 MiB of HBM per device.

v0:
```python
import math
import jax
import jax.numpy as jnp
from jax import lax
from jax.sharding import Mesh
from jax.sharding import PartitionSpec as P

D = 4096
DK = 128
DV = 128
NEW = 4
KV = ("kv_0", "kv_1")
epsilon = 1e-06


def split_up(shard, dim, peers):
    before, after = (shard.shape[:dim], shard.shape[dim + 1 :])
    return jnp.moveaxis(shard.reshape(*before, peers, -1, *after), dim, 0)


def sent_and_summed(shard, axis, dim):
    parts = split_up(shard, dim, lax.axis_size(axis))
    arrived = lax.all_to_all(parts, axis, split_axis=0, concat_axis=0, tiled=True)
    return arrived.astype(jnp.float32).sum(axis=0)


def in_one_piece(arrays, axis, dim, along):
    widths = [math.prod(a.shape[along:]) for a in arrays]
    both = jnp.concatenate(
        [a.reshape(*a.shape[:along], w) for a, w in zip(arrays, widths)], axis=along
    )
    filled = sent_and_summed(both, axis, dim)
    parts = jnp.split(filled, [sum(widths[:k]) for k in range(1, len(widths))], axis=along)
    return tuple(
        (b.reshape(*filled.shape[:along], *a.shape[along:]) for a, b in zip(arrays, parts))
    )


def copy_for_each(shard, axis):
    peers = lax.axis_size(axis)
    return lax.all_to_all(
        jnp.broadcast_to(shard[None], (peers, *shard.shape)), axis, 0, 0, tiled=True
    )


def joined_along(parts, dim):
    parts = jnp.moveaxis(parts, 0, dim)
    dims = parts.shape
    return parts.reshape(*dims[:dim], dims[dim] * dims[dim + 1], *dims[dim + 2 :])


def collect(shard, axis, dim):
    parts = copy_for_each(shard, axis)
    return joined_along(parts, dim)


def of_everyone(shard, axis):
    return copy_for_each(shard, axis).sum(axis=0)


def gather_in_order(shard, axes, order):
    parts = shard[None]
    for k in order:
        parts = lax.all_gather(parts, axes[k], axis=0, tiled=True)
    carried = [lax.axis_size(axes[k]) for k in reversed(order)]
    parts = parts.reshape(*carried, *shard.shape)
    turned = sorted(range(len(order)), key=lambda place: order[len(order) - 1 - place])
    return parts.transpose(*turned, *range(len(order), parts.ndim)).reshape(-1, *shard.shape)


def gather_axes(shard, axes, order, dim):
    return joined_along(gather_in_order(shard, axes, order), dim)


def over_copies(shard, axis):
    everything = copy_for_each(shard, axis)
    return jnp.sum(everything.astype(jnp.float32), axis=0)


def unit_rows(values):
    return values * lax.rsqrt(jnp.sum(values * values, axis=-1, keepdims=True) + epsilon)


def advance(memory, queries, key_rows, value_rows, decays, betas):
    outputs = []
    for step in range(queries.shape[1]):
        memory = jnp.exp(decays[:, step])[:, :, None, None] * memory
        predicted = jnp.einsum(
            "shde,shd->she", memory, key_rows[:, step], precision=lax.Precision.HIGHEST
        )
        correction = betas[:, step][:, :, None] * (value_rows[:, step] - predicted)
        memory = memory + key_rows[:, step][:, :, :, None] * correction[:, :, None, :]
        outputs.append(
            jnp.einsum("shde,shd->she", memory, queries[:, step], precision=lax.Precision.HIGHEST)
        )
    return (memory, jnp.stack(outputs, axis=1))


def per_device(
    tokens,
    lengths,
    memory,
    norm_gain,
    w_query,
    w_key,
    w_value,
    w_outgate,
    w_alpha,
    w_beta,
    decay_log,
    decay_bias,
    head_gain,
    w_output,
    mlp_gain,
    w_gate,
    w_up,
    w_down,
):
    total_rows = tokens.shape[0]
    kv_count = lax.axis_size(KV)
    kv_place = lax.axis_index(KV)
    tp_place = lax.axis_index("tp")
    own_rows = total_rows // kv_count
    seq_dev = memory.shape[0]
    heads_dev = memory.shape[1]
    token_f = tokens.astype(jnp.float32)
    squares = jnp.sum(token_f * token_f, axis=1)
    scaled = (token_f * norm_gain).astype(jnp.bfloat16)
    part_query = jnp.dot(scaled, w_query, preferred_element_type=jnp.float32)
    part_key = jnp.dot(scaled, w_key, preferred_element_type=jnp.float32)
    part_value = jnp.dot(scaled, w_value, preferred_element_type=jnp.float32)
    part_gate = jnp.dot(scaled, w_outgate, preferred_element_type=jnp.float32)
    part_alpha = jnp.dot(scaled, w_alpha, preferred_element_type=jnp.float32)
    part_beta = jnp.dot(scaled, w_beta, preferred_element_type=jnp.float32)
    sum_query, sum_key, sum_value, sum_gate, sum_alpha, sum_beta, own_squares = in_one_piece(
        (
            part_query.astype(jnp.bfloat16),
            part_key.astype(jnp.bfloat16),
            part_value.astype(jnp.bfloat16),
            part_gate.astype(jnp.bfloat16),
            part_alpha.astype(jnp.bfloat16),
            part_beta.astype(jnp.bfloat16),
            squares.astype(jnp.bfloat16),
        ),
        KV,
        0,
        1,
    )
    rstd = lax.rsqrt(own_squares / D + epsilon)[:, None]
    queries = (sum_query * rstd).astype(jnp.bfloat16)
    key_rows = (sum_key * rstd).astype(jnp.bfloat16)
    value_rows = (sum_value * rstd).astype(jnp.bfloat16)
    outgate = (sum_gate * rstd).astype(jnp.bfloat16)
    alphas = lax.dynamic_slice_in_dim(sum_alpha * rstd, tp_place * heads_dev, heads_dev, 1)
    beta_pre = lax.dynamic_slice_in_dim(sum_beta * rstd, tp_place * heads_dev, heads_dev, 1)
    own_lengths = lax.dynamic_slice_in_dim(lengths, kv_place * seq_dev, seq_dev)
    live = jnp.arange(NEW, dtype=jnp.int32)[None, :] < own_lengths[:, None]
    query_h = unit_rows(queries.astype(jnp.float32).reshape(seq_dev, NEW, heads_dev, DK)) * DK ** (
        -0.5
    )
    key_h = unit_rows(key_rows.astype(jnp.float32).reshape(seq_dev, NEW, heads_dev, DK))
    value_h = value_rows.astype(jnp.float32).reshape(seq_dev, NEW, heads_dev, DV)
    decays = -jnp.exp(decay_log) * jax.nn.softplus(alphas + decay_bias)
    decays = jnp.where(live[:, :, None], decays.reshape(seq_dev, NEW, heads_dev), 0.0)
    betas = jnp.where(
        live[:, :, None], jax.nn.sigmoid(beta_pre).reshape(seq_dev, NEW, heads_dev), 0.0
    )
    new_memory, attended = advance(memory, query_h, key_h, value_h, decays, betas)
    attended = attended * lax.rsqrt(jnp.mean(attended * attended, axis=-1, keepdims=True) + epsilon)
    gate_h = outgate.astype(jnp.float32).reshape(seq_dev, NEW, heads_dev, DV)
    mixed = (
        (attended * head_gain * jax.nn.silu(gate_h))
        .astype(jnp.bfloat16)
        .reshape(own_rows, heads_dev * DV)
    )
    attn_terms = jnp.dot(collect(mixed, KV, 0), w_output, preferred_element_type=jnp.float32)
    attn_total = of_everyone(attn_terms, "tp")
    hidden = (token_f + attn_total).astype(jnp.bfloat16)
    hidden_f = hidden.astype(jnp.float32)
    hidden_squares = jnp.sum(hidden_f * hidden_f, axis=1)
    hscaled = (hidden_f * mlp_gain).astype(jnp.bfloat16)
    all_live = (jnp.arange(NEW, dtype=jnp.int32)[None, :] < lengths[:, None]).reshape(total_rows)
    part_gate_rows = jnp.dot(hscaled, w_gate, preferred_element_type=jnp.float32)
    part_up_rows = jnp.dot(hscaled, w_up, preferred_element_type=jnp.float32)
    gate_rows, up_rows, mlp_squares = in_one_piece(
        (
            part_gate_rows.astype(jnp.bfloat16),
            part_up_rows.astype(jnp.bfloat16),
            hidden_squares.astype(jnp.bfloat16),
        ),
        KV,
        0,
        1,
    )
    rstd2 = lax.rsqrt(mlp_squares / D + epsilon)[:, None]
    active = (jax.nn.silu(gate_rows * rstd2) * (up_rows * rstd2)).astype(jnp.bfloat16)
    feed_terms = jnp.dot(
        gather_axes(active, KV, (0, 1), 0), w_down, preferred_element_type=jnp.float32
    )
    feed_total = over_copies(feed_terms.astype(jnp.bfloat16), "tp").astype(jnp.float32)
    layer_out = jnp.where(all_live[:, None], hidden_f + feed_total, 0.0).astype(jnp.bfloat16)
    return (layer_out, new_memory)


def solution(mesh):
    torus = Mesh(mesh.devices.reshape(16, 4, mesh.shape["tp"]), ("kv_0", "kv_1", "tp"))
    placed = (
        P(None, KV),
        P(),
        P(KV, "tp", None, None),
        P(KV),
        P(KV, "tp"),
        P(KV, "tp"),
        P(KV, "tp"),
        P(KV, "tp"),
        P(KV, None),
        P(KV, None),
        P("tp"),
        P("tp"),
        P(),
        P("tp", KV),
        P(KV),
        P(KV, "tp"),
        P(KV, "tp"),
        P("tp", KV),
    )
    return jax.shard_map(
        per_device,
        mesh=torus,
        in_specs=placed,
        out_specs=(P(None, KV), P(KV, "tp", None, None)),
        check_vma=False,
    )
```

profile of v0, /device:TPU:1, one launch (start us, length us, event | category | flops | bytes accessed | tf_op | source)
XLA Modules:
  0.0 242.6 jit_solution(11514970106353623751)
XLA Ops:
  0.7 0.8 fusion.21
  1.5 1.1 convolution_convert_fusion.5
  2.6 1.1 convolution_convert_fusion.4
  3.8 1.1 convolution_convert_fusion.3
  4.9 1.1 convolution_convert_fusion.2
  7.0 2.5 %concatenate.42 = bf16[64,4,1057]{2,1,0:T(4,128)(2,1)} concatenate(bf16[64,4,256]{2,1,0:T(4,128)(2,1)S(1)} %concatenate.36, bf16[64,4,256]{2,1,0:T(4,128)(2,1)S(1)} %concatenate.37, bf16[64,4,256]{2,1,0:T(4,128)(2,1)S(1)} %concatenate.38, bf16[64,4,256]{2,1,0:T(4,128)(2,1)S(1)} %concatenate.39, bf16[64,4,16]{2,1,0:T(4,128)(2,1)S(1)} %bitcast.169, ...), dimensions={2} | concatenate | bytes 1082368 | tf_op jit(solution)/shard_map/concatenate | solution.py:29
  9.5 19.3 %all-to-all-start = ((bf16[64,4,1057]{2,1,0:T(4,128)(2,1)}), bf16[64,4,1057]{2,1,0:T(4,128)(2,1)S(1)}, u32[]{:S(2)}, u32[]{:S(2)}) async-start(bf16[64,4,1057]{2,1,0:T(4,128)(2,1)} %concatenate.42), calls=%async_computation | async-start | bytes 1179648 | tf_op jit(solution)/shard_map/all_to_all | solution.py:23
  28.8 0.6 dynamic_slice.9
  29.4 0.6 iota_compare_fusion.1
  30.1 31.9 %all-to-all-done = bf16[64,4,1057]{2,1,0:T(4,128)(2,1)S(1)} async-done(((bf16[64,4,1057]{2,1,0:T(4,128)(2,1)}), bf16[64,4,1057]{2,1,0:T(4,128)(2,1)S(1)}, u32[]{:S(2)}, u32[]{:S(2)}) %all-to-all-start) | async-done | bytes 541216 | tf_op jit(solution)/shard_map/all_to_all | solution.py:23
  67.1 22.2 %all_to_all.25 = bf16[64,4,256]{2,1,0:T(4,128)(2,1)S(1)} all-to-all(bf16[64,4,256]{2,1,0:T(4,128)(2,1)S(1)} %broadcast_in_dim.32), channel_id=1, replica_groups=mesh['kv_0'=16,'kv_1'=4,'tp'=8] {'kv_0','kv_1'}, dimensions={0} | all-to-all | bytes 262144 | tf_op jit(solution)/shard_map/all_to_all | solution.py:41
  89.6 17.0 %all_to_all.26 = f32[8,256,64]{1,2,0:T(8,128)S(1)} all-to-all(f32[8,256,64]{1,2,0:T(8,128)S(1)} %broadcast_in_dim.33), channel_id=1, replica_groups=mesh['kv_0'=16,'kv_1'=4,'tp'=8] {'tp'}, dimensions={0} | all-to-all | bytes 1048576 | tf_op jit(solution)/shard_map/all_to_all | solution.py:41
  106.7 0.4 convolution_convert_fusion.1
  107.6 0.4 convolution_convert_fusion
  108.4 0.7 pad_maximum_fusion
  109.1 74.8 %all_to_all.27 = bf16[64,4,2817]{2,1,0:T(4,128)(2,1)S(1)} all-to-all(bf16[64,4,2817]{2,1,0:T(4,128)(2,1)S(1)} %pad_maximum_fusion), channel_id=1, replica_groups=mesh['kv_0'=16,'kv_1'=4,'tp'=8] {'kv_0','kv_1'}, dimensions={0} | all-to-all | bytes 2884608 | tf_op jit(solution)/shard_map/all_to_all | solution.py:23
  183.9 0.6 convert_reduce_fusion
  184.8 22.4 %all-gather.1 = bf16[16,4,1408]{2,1,0:T(4,128)(2,1)S(1)} all-gather(bf16[1,4,1408]{2,1,0:T(4,128)(2,1)S(1)} %fusion.47), channel_id=2, replica_groups=mesh['kv_0'=16,'kv_1'=4,'tp'=8] {'kv_0'}, dimensions={0}, use_global_device_ids=true | all-gather | bytes 191488 | tf_op jit(solution)/shard_map/all_gather | solution.py:64
  207.1 10.5 %all_gather.7 = bf16[64,4,1408]{2,1,0:T(4,128)(2,1)S(1)} all-gather(bf16[16,4,1408]{2,1,0:T(4,128)(2,1)S(1)} %all-gather.1), channel_id=1, replica_groups=mesh['kv_0'=16,'kv_1'=4,'tp'=8] {'kv_1'}, dimensions={0}, use_global_device_ids=true | all-gather | bytes 901120 | tf_op jit(solution)/shard_map/all_gather | solution.py:64
  218.1 0.5 copy-done.4
  219.0 0.7 broadcast_in_dim.35
  219.7 15.8 %all-to-all-start.4 = ((bf16[8,256,64]{1,2,0:T(8,128)(2,1)}), bf16[8,256,64]{1,2,0:T(8,128)(2,1)S(1)}, u32[]{:S(2)}, u32[]{:S(2)}) async-start(bf16[8,256,64]{1,2,0:T(8,128)(2,1)} %broadcast_in_dim.35), calls=%async_computation.4 | async-start | bytes 524288 | tf_op jit(solution)/shard_map/all_to_all | solution.py:41
  235.6 6.3 %all-to-all-done.4 = bf16[8,256,64]{1,2,0:T(8,128)(2,1)S(1)} async-done(((bf16[8,256,64]{1,2,0:T(8,128)(2,1)}), bf16[8,256,64]{1,2,0:T(8,128)(2,1)S(1)}, u32[]{:S(2)}, u32[]{:S(2)}) %all-to-all-start.4) | async-done | bytes 262176 | tf_op jit(solution)/shard_map/all_to_all | solution.py:41
  242.0 0.6 fusion.26
  (95 shorter events, 8.5 us)
Async XLA Ops:
  0.6 106.1 %copy-start = (bf16[64,1408]{1,0:T(8,128)(2,1)S(1)}, bf16[64,1408]{1,0:T(8,128)(2,1)}, u32[]{:S(2)}) copy-start(bf16[64,1408]{1,0:T(8,128)(2,1)} %param.33) | copy-start | bytes 540676
  0.6 5.4 %copy-start.2 = (bf16[256,64]{0,1:T(8,128)(2,1)S(1)}, bf16[256,64]{0,1:T(8,128)(2,1)}, u32[]{:S(2)}) copy-start(bf16[256,64]{0,1:T(8,128)(2,1)} %param.18) | copy-start | bytes 98308
  0.7 5.4 %copy-start.7 = (f32[64]{0:T(128)S(1)}, f32[64]{0:T(128)}, u32[]{:S(2)}) copy-start(f32[64]{0:T(128)} %param.21) | copy-start | bytes 772
  0.7 5.4 %copy-start.11 = (bf16[64,16]{0,1:T(8,128)(2,1)S(1)}, bf16[64,16]{0,1:T(8,128)(2,1)}, u32[]{:S(2)}) copy-start(bf16[64,16]{0,1:T(8,128)(2,1)} %param.26) | copy-start | bytes 6148
  0.7 5.7 %copy-start.12 = (bf16[64,16]{0,1:T(8,128)(2,1)S(1)}, bf16[64,16]{0,1:T(8,128)(2,1)}, u32[]{:S(2)}) copy-start(bf16[64,16]{0,1:T(8,128)(2,1)} %param.27) | copy-start | bytes 6148
  6.0 22.8 %copy-start.10 = (s32[64]{0:T(128)S(1)}, s32[64]{0:T(128)}, u32[]{:S(2)}) copy-start(s32[64]{0:T(128)} %param.19) | copy-start | bytes 772
  6.0 24.1 %copy-start.13 = (f32[2]{0:T(128)S(1)}, f32[2]{0:T(128)}, u32[]{:S(2)}) copy-start(f32[2]{0:T(128)} %param.28) | copy-start | bytes 28
  6.0 24.1 %copy-start.14 = (f32[128]{0:T(128)S(1)}, f32[128]{0:T(128)}, u32[]{:S(2)}) copy-start(f32[128]{0:T(128)} %param.30) | copy-start | bytes 1540
  7.0 55.6 %copy-start.9 = (f32[2]{0:T(128)S(1)}, f32[2]{0:T(128)}, u32[]{:S(2)}) copy-start(f32[2]{0:T(128)} %param.29) | copy-start | bytes 28
  7.0 56.8 %copy-start.1 = (f32[1,2,128,128]{3,2,1,0:T(8,128)S(1)}, f32[1,2,128,128]{3,2,1,0:T(8,128)}, u32[]{:S(2)}) copy-start(f32[1,2,128,128]{3,2,1,0:T(8,128)} %param.20) | copy-start | bytes 393220
  9.5 52.5 %all-to-all-start = ((bf16[64,4,1057]{2,1,0:T(4,128)(2,1)}), bf16[64,4,1057]{2,1,0:T(4,128)(2,1)S(1)}, u32[]{:S(2)}, u32[]{:S(2)}) async-start(bf16[64,4,1057]{2,1,0:T(4,128)(2,1)} %concatenate.42), calls=%async_computation | async-start | bytes 1179648 | tf_op jit(solution)/shard_map/all_to_all | solution.py:23
  30.1 59.3 %copy-start.6 = (bf16[256,64]{0,1:T(8,128)(2,1)S(1)}, bf16[256,64]{0,1:T(8,128)(2,1)}, u32[]{:S(2)}) copy-start(bf16[256,64]{0,1:T(8,128)(2,1)} %param.31) | copy-start | bytes 98308
  66.5 40.1 %copy-start.3 = (f32[1,2,128,128]{3,2,1,0:T(8,128)}, f32[1,2,128,128]{3,2,1,0:T(8,128)S(1)}, u32[]{:S(2)}) copy-start(f32[1,2,128,128]{3,2,1,0:T(8,128)S(1)} %multiply_add_fusion) | copy-start | bytes 393220
  67.1 39.6 %copy-start.8 = (f32[64]{0:T(128)S(1)}, f32[64]{0:T(128)}, u32[]{:S(2)}) copy-start(f32[64]{0:T(128)} %param.32) | copy-start | bytes 772
  106.6 0.9 copy-start.5
  217.7 0.9 copy-start.4
  219.7 22.3 %all-to-all-start.4 = ((bf16[8,256,64]{1,2,0:T(8,128)(2,1)}), bf16[8,256,64]{1,2,0:T(8,128)(2,1)S(1)}, u32[]{:S(2)}, u32[]{:S(2)}) async-start(bf16[8,256,64]{1,2,0:T(8,128)(2,1)} %broadcast_in_dim.35), calls=%async_computation.4 | async-start | bytes 524288 | tf_op jit(solution)/shard_map/all_to_all | solution.py:41
where the time goes:
time: 243 us
  blocking collectives  147 us (60%)
  waiting for transfers between devices  38.2 us (16%)
  starting transfers between devices  35 us (14%)
  matrix products  8.38 us (3%)
  local copies, waits for them, and re-layouts  7.27 us (3%)
  other arithmetic  5.71 us (2%)
    all_to_all x1, blocking collectives, sent_and_summed(): lax.all_to_all(parts, axis, split_axis=0, concat_axis=0, tiled=True)  74.8 us
    all_to_all x2, blocking collectives, copy_for_each(): lax.all_to_all(jnp.broadcast_to(shard[None], (peers, *shard.shape)), axis...  39.2 us
    all_gather x2, blocking collectives, gather_in_order(): parts = lax.all_gather(parts, axes[k], axis=0, tiled=True)  32.9 us
    all_to_all x1, waiting for transfers between devices, sent_and_summed(): lax.all_to_all(parts, axis, split_axis=0, concat_axis=0, tiled=True)  31.9 us
    all_to_all x1, starting transfers between devices, sent_and_summed(): lax.all_to_all(parts, axis, split_axis=0, concat_axis=0, tiled=True)  19.3 us
    all_to_all x1, starting transfers between devices, copy_for_each(): lax.all_to_all(jnp.broadcast_to(shard[None], (peers, *shard.shape)), axis...  15.8 us
    all_to_all x1, waiting for transfers between devices, copy_for_each(): lax.all_to_all(jnp.broadcast_to(shard[None], (peers, *shard.shape)), axis...  6.3 us
  transfers between devices with their start and end apart: 2, of which 2 were waited for; matrix products, arithmetic and copies ran while one was open for 1% of the time, Pallas kernels for 0%

commit v1 on v0

--- a/solution.py
+++ b/solution.py
@@ -61,7 +61,8 @@
 def gather_in_order(shard, axes, order):
     parts = shard[None]
     for k in order:
-        parts = lax.all_gather(parts, axes[k], axis=0, tiled=True)
+        repeated = jnp.stack([parts] * lax.axis_size(axes[k]))
+        parts = jnp.concatenate(lax.all_to_all(repeated, axes[k], 0, 0), axis=0)
     carried = [lax.axis_size(axes[k]) for k in reversed(order)]
     parts = parts.reshape(*carried, *shard.shape)
     turned = sorted(range(len(order)), key=lambda place: order[len(order) - 1 - place])

time: 243 us -> 234 us (0.963)
  starting transfers between devices: 35 us -> 29.1 us
  blocking collectives: 147 us -> 143 us
    all_gather x2 -> x0, blocking collectives: 32.9 us -> none  [gather_in_order(): parts = lax.all_gather(parts, axes[k], axis=0, tiled=True)]
    all_to_all x0 -> x2, blocking collectives: none -> 29.3 us  [gather_in_order(): parts = jnp.concatenate(lax.all_to_all(repeated, axes[k], 0, 0), axis=0)]
    all_to_all x1, starting transfers between devices: 15.8 us -> 9.86 us  [copy_for_each(): lax.all_to_all(jnp.broadcast_to(shard[None], (peers, *shard.shape)), axis...]
where the time goes in v1:
time: 234 us; the launch traced here: 233 us
  blocking collectives  143 us (61%)
  waiting for transfers between devices  38.2 us (16%)
  starting transfers between devices  29.1 us (12%)
  matrix products  8.38 us (4%)
  local copies, waits for them, and re-layouts  7.51 us (3%)
  other arithmetic  5.71 us (2%)
    all_to_all x1, blocking collectives, sent_and_summed(): lax.all_to_all(parts, axis, split_axis=0, concat_axis=0, tiled=True)  74.8 us
    all_to_all x2, blocking collectives, copy_for_each(): lax.all_to_all(jnp.broadcast_to(shard[None], (peers, *shard.shape)), axis...  39.2 us
    all_to_all x1, waiting for transfers between devices, sent_and_summed(): lax.all_to_all(parts, axis, split_axis=0, concat_axis=0, tiled=True)  31.9 us
    all_to_all x2, blocking collectives, gather_in_order(): parts = jnp.concatenate(lax.all_to_all(repeated, axes[k], 0, 0), axis=0)  29.3 us
    all_to_all x1, starting transfers between devices, sent_and_summed(): lax.all_to_all(parts, axis, split_axis=0, concat_axis=0, tiled=True)  19.3 us
    all_to_all x1, starting transfers between devices, copy_for_each(): lax.all_to_all(jnp.broadcast_to(shard[None], (peers, *shard.shape)), axis...  9.86 us
    all_to_all x1, waiting for transfers between devices, copy_for_each(): lax.all_to_all(jnp.broadcast_to(shard[None], (peers, *shard.shape)), axis...  6.3 us
  transfers between devices with their start and end apart: 2, of which 2 were waited for; matrix products, arithmetic and copies ran while one was open for 1% of the time, Pallas kernels for 0%

profile of v1, /device:TPU:1, one launch (start us, length us, event | category | flops | bytes accessed | tf_op | source)
XLA Modules:
  0.0 233.3 jit_solution(2478188476009651068)
XLA Ops:
  0.7 0.8 fusion.21
  1.5 1.1 convolution_convert_fusion.5
  2.6 1.1 convolution_convert_fusion.4
  3.8 1.1 convolution_convert_fusion.3
  4.9 1.1 convolution_convert_fusion.2
  7.0 2.5 %concatenate.42 = bf16[64,4,1057]{2,1,0:T(4,128)(2,1)} concatenate(bf16[64,4,256]{2,1,0:T(4,128)(2,1)S(1)} %concatenate.36, bf16[64,4,256]{2,1,0:T(4,128)(2,1)S(1)} %concatenate.37, bf16[64,4,256]{2,1,0:T(4,128)(2,1)S(1)} %concatenate.38, bf16[64,4,256]{2,1,0:T(4,128)(2,1)S(1)} %concatenate.39, bf16[64,4,16]{2,1,0:T(4,128)(2,1)S(1)} %bitcast.165, ...), dimensions={2} | concatenate | bytes 1082368 | tf_op jit(solution)/shard_map/concatenate | solution.py:29
  9.5 19.3 %all-to-all-start = ((bf16[64,4,1057]{2,1,0:T(4,128)(2,1)}), bf16[64,4,1057]{2,1,0:T(4,128)(2,1)S(1)}, u32[]{:S(2)}, u32[]{:S(2)}) async-start(bf16[64,4,1057]{2,1,0:T(4,128)(2,1)} %concatenate.42), calls=%async_computation | async-start | bytes 1179648 | tf_op jit(solution)/shard_map/all_to_all | solution.py:23
  28.8 0.6 dynamic_slice.9
  29.4 0.6 iota_compare_fusion.1
  30.1 31.9 %all-to-all-done = bf16[64,4,1057]{2,1,0:T(4,128)(2,1)S(1)} async-done(((bf16[64,4,1057]{2,1,0:T(4,128)(2,1)}), bf16[64,4,1057]{2,1,0:T(4,128)(2,1)S(1)}, u32[]{:S(2)}, u32[]{:S(2)}) %all-to-all-start) | async-done | bytes 541216 | tf_op jit(solution)/shard_map/all_to_all | solution.py:23
  67.1 22.2 %all_to_all.35 = bf16[64,4,256]{2,1,0:T(4,128)(2,1)S(1)} all-to-all(bf16[64,4,256]{2,1,0:T(4,128)(2,1)S(1)} %broadcast_in_dim.30), channel_id=1, replica_groups=mesh['kv_0'=16,'kv_1'=4,'tp'=8] {'kv_0','kv_1'}, dimensions={0} | all-to-all | bytes 262144 | tf_op jit(solution)/shard_map/all_to_all | solution.py:41
  89.6 17.0 %all_to_all.36 = f32[8,256,64]{1,2,0:T(8,128)S(1)} all-to-all(f32[8,256,64]{1,2,0:T(8,128)S(1)} %broadcast_in_dim.31), channel_id=1, replica_groups=mesh['kv_0'=16,'kv_1'=4,'tp'=8] {'tp'}, dimensions={0} | all-to-all | bytes 1048576 | tf_op jit(solution)/shard_map/all_to_all | solution.py:41
  106.7 0.4 convolution_convert_fusion.1
  107.6 0.4 convolution_convert_fusion
  108.4 0.7 pad_maximum_fusion
  109.1 74.8 %all_to_all.37 = bf16[64,4,2817]{2,1,0:T(4,128)(2,1)S(1)} all-to-all(bf16[64,4,2817]{2,1,0:T(4,128)(2,1)S(1)} %pad_maximum_fusion), channel_id=1, replica_groups=mesh['kv_0'=16,'kv_1'=4,'tp'=8] {'kv_0','kv_1'}, dimensions={0} | all-to-all | bytes 2884608 | tf_op jit(solution)/shard_map/all_to_all | solution.py:23
  183.9 0.6 convert_reduce_fusion
  184.8 18.1 %all_to_all.38 = bf16[16,1,4,1408]{3,2,1,0:T(4,128)(2,1)S(1)} all-to-all(bf16[16,1,4,1408]{3,2,1,0:T(4,128)(2,1)S(1)} %stack.41), channel_id=1, replica_groups=mesh['kv_0'=16,'kv_1'=4,'tp'=8] {'kv_0'}, dimensions={0} | all-to-all | bytes 360448 | tf_op jit(solution)/shard_map/all_to_all | solution.py:65
  203.1 11.2 %all_to_all.39 = bf16[4,16,4,1408]{3,2,1,0:T(4,128)(2,1)S(1)} all-to-all(bf16[4,16,4,1408]{3,2,1,0:T(4,128)(2,1)S(1)} %stack.42), channel_id=1, replica_groups=mesh['kv_0'=16,'kv_1'=4,'tp'=8] {'kv_1'}, dimensions={0} | all-to-all | bytes 1441792 | tf_op jit(solution)/shard_map/all_to_all | solution.py:65
  214.7 0.5 copy-done.4
  215.6 0.7 broadcast_in_dim.32
  216.3 9.9 %all-to-all-start.6 = ((bf16[8,256,64]{1,2,0:T(8,128)(2,1)}), bf16[8,256,64]{1,2,0:T(8,128)(2,1)S(1)}, u32[]{:S(2)}, u32[]{:S(2)}) async-start(bf16[8,256,64]{1,2,0:T(8,128)(2,1)} %broadcast_in_dim.32), calls=%async_computation.6 | async-start | bytes 524288 | tf_op jit(solution)/shard_map/all_to_all | solution.py:41
  226.4 6.3 %all-to-all-done.6 = bf16[8,256,64]{1,2,0:T(8,128)(2,1)S(1)} async-done(((bf16[8,256,64]{1,2,0:T(8,128)(2,1)}), bf16[8,256,64]{1,2,0:T(8,128)(2,1)S(1)}, u32[]{:S(2)}, u32[]{:S(2)}) %all-to-all-start.6) | async-done | bytes 262176 | tf_op jit(solution)/shard_map/all_to_all | solution.py:41
  232.7 0.6 fusion.26
  (97 shorter events, 8.7 us)
Async XLA Ops:
  0.6 106.1 %copy-start = (bf16[64,1408]{1,0:T(8,128)(2,1)S(1)}, bf16[64,1408]{1,0:T(8,128)(2,1)}, u32[]{:S(2)}) copy-start(bf16[64,1408]{1,0:T(8,128)(2,1)} %param.33) | copy-start | bytes 540676
  0.6 5.4 %copy-start.2 = (bf16[256,64]{0,1:T(8,128)(2,1)S(1)}, bf16[256,64]{0,1:T(8,128)(2,1)}, u32[]{:S(2)}) copy-start(bf16[256,64]{0,1:T(8,128)(2,1)} %param.18) | copy-start | bytes 98308
  0.7 5.4 %copy-start.7 = (f32[64]{0:T(128)S(1)}, f32[64]{0:T(128)}, u32[]{:S(2)}) copy-start(f32[64]{0:T(128)} %param.21) | copy-start | bytes 772
  0.7 5.4 %copy-start.11 = (bf16[64,16]{0,1:T(8,128)(2,1)S(1)}, bf16[64,16]{0,1:T(8,128)(2,1)}, u32[]{:S(2)}) copy-start(bf16[64,16]{0,1:T(8,128)(2,1)} %param.26) | copy-start | bytes 6148
  0.7 5.7 %copy-start.12 = (bf16[64,16]{0,1:T(8,128)(2,1)S(1)}, bf16[64,16]{0,1:T(8,128)(2,1)}, u32[]{:S(2)}) copy-start(bf16[64,16]{0,1:T(8,128)(2,1)} %param.27) | copy-start | bytes 6148
  6.0 22.8 %copy-start.10 = (s32[64]{0:T(128)S(1)}, s32[64]{0:T(128)}, u32[]{:S(2)}) copy-start(s32[64]{0:T(128)} %param.19) | copy-start | bytes 772
  6.0 24.1 %copy-start.13 = (f32[2]{0:T(128)S(1)}, f32[2]{0:T(128)}, u32[]{:S(2)}) copy-start(f32[2]{0:T(128)} %param.28) | copy-start | bytes 28
  6.0 24.1 %copy-start.14 = (f32[128]{0:T(128)S(1)}, f32[128]{0:T(128)}, u32[]{:S(2)}) copy-start(f32[128]{0:T(128)} %param.30) | copy-start | bytes 1540
  7.0 55.6 %copy-start.9 = (f32[2]{0:T(128)S(1)}, f32[2]{0:T(128)}, u32[]{:S(2)}) copy-start(f32[2]{0:T(128)} %param.29) | copy-start | bytes 28
  7.0 56.8 %copy-start.1 = (f32[1,2,128,128]{3,2,1,0:T(8,128)S(1)}, f32[1,2,128,128]{3,2,1,0:T(8,128)}, u32[]{:S(2)}) copy-start(f32[1,2,128,128]{3,2,1,0:T(8,128)} %param.20) | copy-start | bytes 393220
  9.5 52.5 %all-to-all-start = ((bf16[64,4,1057]{2,1,0:T(4,128)(2,1)}), bf16[64,4,1057]{2,1,0:T(4,128)(2,1)S(1)}, u32[]{:S(2)}, u32[]{:S(2)}) async-start(bf16[64,4,1057]{2,1,0:T(4,128)(2,1)} %concatenate.42), calls=%async_computation | async-start | bytes 1179648 | tf_op jit(solution)/shard_map/all_to_all | solution.py:23
  30.1 59.3 %copy-start.6 = (bf16[256,64]{0,1:T(8,128)(2,1)S(1)}, bf16[256,64]{0,1:T(8,128)(2,1)}, u32[]{:S(2)}) copy-start(bf16[256,64]{0,1:T(8,128)(2,1)} %param.31) | copy-start | bytes 98308
  66.5 40.1 %copy-start.3 = (f32[1,2,128,128]{3,2,1,0:T(8,128)}, f32[1,2,128,128]{3,2,1,0:T(8,128)S(1)}, u32[]{:S(2)}) copy-start(f32[1,2,128,128]{3,2,1,0:T(8,128)S(1)} %multiply_add_fusion) | copy-start | bytes 393220
  67.1 39.6 %copy-start.8 = (f32[64]{0:T(128)S(1)}, f32[64]{0:T(128)}, u32[]{:S(2)}) copy-start(f32[64]{0:T(128)} %param.32) | copy-start | bytes 772
  106.6 0.9 copy-start.5
  214.3 0.9 copy-start.4
  216.3 16.4 %all-to-all-start.6 = ((bf16[8,256,64]{1,2,0:T(8,128)(2,1)}), bf16[8,256,64]{1,2,0:T(8,128)(2,1)S(1)}, u32[]{:S(2)}, u32[]{:S(2)}) async-start(bf16[8,256,64]{1,2,0:T(8,128)(2,1)} %broadcast_in_dim.32), calls=%async_computation.6 | async-start | bytes 524288 | tf_op jit(solution)/shard_map/all_to_all | solution.py:41
